TPU v7x, 32 devices: a whole 2x2x4 slice. The times are simulated.
32 devices in a mesh: sp: 4 (over z), fs: 4 (over y, x), tp: 2 (over core).
Axes of the slice: x: 2, y: 2, z: 4, core: 2. Of those that a mesh axis runs over, the one named last changes fastest.
Arguments:
- tokens: bfloat16 [1024, 2048], P(('sp', 'fs', 'tp')), may hold values from -6 to 6
- norm_gain: float32 [2048], replicated, may hold values from 0.1 to 1.9
- w_query: bfloat16 [2048, 1024], P(None, ('fs', 'tp')), may hold values from -0.125 to 0.125
- w_key: bfloat16 [2048, 1024], P(None, ('fs', 'tp')), may hold values from -0.125 to 0.125
- w_value: bfloat16 [2048, 1024], P(None, ('fs', 'tp')), may hold values from -0.125 to 0.125
- w_pool: bfloat16 [2048, 1024], P(None, ('fs', 'tp')), may hold values from -0.125 to 0.125
- query_gain: float32 [64], replicated, may hold values from 1.2 to 1.6
- key_gain: float32 [64], replicated, may hold values from 1.2 to 1.6
- lambdas: float32 [8], P(('fs', 'tp')), may hold values from 0.3 to 0.8
- head_gain: float32 [128], replicated, may hold values from 0.1 to 1.9
- w_out_attn: bfloat16 [1024, 2048], P(('fs', 'tp')), may hold values from -0.125 to 0.125
- w_out_pool: bfloat16 [1024, 2048], P(('fs', 'tp')), may hold values from -0.125 to 0.125
Outputs:
- layer_out: bfloat16 [1024, 2048], P(('sp', 'fs', 'tp'))
All inputs are finite; a program needn't handle non-finite values.
Results may differ from a plain program's by a relative error of at most 0.015.
Values may be sent and summed in bfloat16 or wider, within the bound.
A program may use at most 128 MiB of HBM per device.

v0:
```python
import functools

import jax
import jax.numpy as jnp
from jax import lax
from jax.experimental import pallas as pl
from jax.experimental.pallas import tpu as pltpu
from jax.sharding import PartitionSpec as P

HEAD_DIM = 64
POOL_GROUP_DIM = 256
HALO = 16
EPS = 1e-06
MESH = pl.DeviceIdType.MESH
F32 = jnp.float32
BF16 = jnp.bfloat16


def kernel(
    n_sp, n_fs, col_chunks,
    tokens_hbm, norm_gain_ref, wq_hbm, wk_hbm, wv_hbm, wp_hbm, query_gain_ref, key_gain_ref,
    lambdas_ref, head_gain_ref, woa_hbm, wop_hbm,
    out_ref,
    tok, gathered, win, wout, kv, qhat, pin, halo_src, halo, numer, total, merged,
    part_send, part_recv, chip_own, chip_send, chip_relay, chip_recv,
    tok_sem, win_sem, wout_sem, ag_send, ag_recv, fwd_send, fwd_recv, kv_send, kv_recv,
    halo_send, halo_recv, a_send, a_recv, b_send, b_recv,
):
    s = lax.axis_index("sp")
    f = lax.axis_index("fs")
    t = lax.axis_index("tp")
    mate = (s, f, 1 - t)
    rows, width = tok.shape
    chip_rows = 2 * rows
    own_rows = n_fs * chip_rows
    heads = lambdas_ref.shape[0]
    qc = wq_hbm.shape[1]
    vc = wv_hbm.shape[1]
    pc = wp_hbm.shape[1]
    v_dim = head_gain_ref.shape[1]
    pair = 2 * HEAD_DIM

    def peer(k):
        return lax.rem(f + k, n_fs)

    fx = f + 1 - 2 * lax.rem(f, 2)
    fy = lax.rem(f + 2, n_fs)
    chips = (f, fx, fy, lax.rem(fx + 2, n_fs))

    tok_copy = pltpu.make_async_copy(tokens_hbm, tok, tok_sem)
    tok_copy.start()
    barrier = pltpu.get_barrier_semaphore()
    pl.semaphore_signal(barrier, inc=1, device_id=mate, device_id_type=MESH)
    for chip in (fx, fy):
        pl.semaphore_signal(barrier, inc=1, device_id=(s, chip, t), device_id_type=MESH)

    @pl.when(s > 0)
    def _():
        pl.semaphore_signal(barrier, inc=1, device_id=(s - 1, f, t), device_id_type=MESH)

    @pl.when(s < n_sp - 1)
    def _():
        pl.semaphore_signal(barrier, inc=1, device_id=(s + 1, f, t), device_id_type=MESH)

    win_copies = []
    at = 0
    for i, (w, c) in enumerate(((wk_hbm, qc), (wv_hbm, vc), (wq_hbm, qc), (wp_hbm, pc))):
        win_copies.append(pltpu.make_async_copy(w, win.at[:, pl.ds(at, c)], win_sem.at[i]))
        at += c
    wout_copies = [
        pltpu.make_async_copy(woa_hbm, wout.at[pl.ds(0, vc), :], wout_sem.at[0]),
        pltpu.make_async_copy(wop_hbm, wout.at[pl.ds(vc, pc), :], wout_sem.at[1]),
    ]
    for c in win_copies + wout_copies:
        c.start()

    tok_copy.wait()
    x = tok[...].astype(F32)
    x = x * lax.rsqrt(jnp.mean(x * x, axis=-1, keepdims=True) + EPS) * norm_gain_ref[...]
    gathered[f, t] = x.astype(BF16).reshape(2, rows // 2, width)

    pl.semaphore_wait(
        barrier, 3 + jnp.where(s > 0, 1, 0) + jnp.where(s < n_sp - 1, 1, 0)
    )

    def along(way, i, chip, half):
        slot = gathered.at[chip, t, half]
        return pltpu.make_async_remote_copy(
            slot, slot, ag_send.at[way, i], ag_recv.at[way, i],
            device_id=(s, (fx, fy)[way], t), device_id_type=MESH,
        )

    own = [[along(way, half, f, half) for half in range(2)] for way in range(2)]
    for way, half in ((0, 1), (1, 0), (0, 0), (1, 1)):
        own[way][half].start()
    far = [along(0, 2, fy, 0), along(1, 2, fx, 1)]

    def across(k, half):
        slot = gathered.at[chips[k], t, half]
        return pltpu.make_async_remote_copy(
            slot, slot, fwd_send.at[k, half], fwd_recv.at[k, half],
            device_id=mate, device_id_type=MESH,
        )

    forwards = [[across(k, half) for half in range(2)] for k in range(n_fs)]
    for c in forwards[0]:
        c.start()

    lane = lax.broadcasted_iota(jnp.int32, (chip_rows, pair), 1)
    low = lane < HEAD_DIM

    def norm_pair(raw, gain):
        sq = raw * raw
        first = jnp.sum(jnp.where(low, sq, 0.0), axis=-1, keepdims=True) * (1.0 / HEAD_DIM)
        second = jnp.sum(jnp.where(low, 0.0, sq), axis=-1, keepdims=True) * (1.0 / HEAD_DIM)
        return raw * jnp.where(low, lax.rsqrt(first + EPS), lax.rsqrt(second + EPS)) * gain

    qg = jnp.concatenate([query_gain_ref[...]] * 2, axis=1)
    kg = jnp.concatenate([key_gain_ref[...]] * 2, axis=1)

    last = n_fs - 1

    def kv_copy(j, k):
        slot = kv.at[j, chips[k]]
        return pltpu.make_async_remote_copy(
            slot, slot, kv_send.at[j, k], kv_recv.at[j, k],
            device_id=(s + 1, f, t), device_id_type=MESH,
        )

    def relay(d, k):
        @pl.when(s >= d)
        def _():
            c = kv_copy(s - d, k)
            c.wait_recv()

            @pl.when(s < n_sp - 1)
            def _():
                c.start()

    for k in range(n_fs):
        chip = chips[k]
        if k == 1:
            own[1][0].wait_recv()
            far[0].start()
            forwards[2][0].start()
            own[0][1].wait_recv()
            far[1].start()
            forwards[1][1].start()
            own[0][0].wait_recv()
            forwards[1][0].start()
            own[1][1].wait_recv()
            forwards[2][1].start()
        if k == last:
            for half in range(2):
                far[half].wait_recv()
                forwards[last][half].start()
            relay(1, 0)
        for c in forwards[k]:
            c.wait_recv()
        if k == 0:
            for c in win_copies:
                c.wait()
        block = gathered[chip].reshape(chip_rows, width)
        proj = jnp.dot(block, win[...], preferred_element_type=F32)
        for h in range(heads):
            kv[s, chip, :, h * pair : (h + 1) * pair] = norm_pair(
                proj[:, h * pair : (h + 1) * pair], kg
            ).astype(BF16)
        kv[s, chip, :, qc : qc + vc] = proj[:, qc : qc + vc].astype(BF16)

        @pl.when(s < n_sp - 1)
        def _(k=k):
            kv_copy(s, k).start()

        for h in range(heads):
            at = qc + vc + h * pair
            q = norm_pair(proj[:, at : at + pair], qg)
            q = q.astype(BF16).astype(F32) * HEAD_DIM ** (-0.5)
            qhat[h, 0, chip] = jnp.where(low, q, 0.0).astype(BF16)
            qhat[h, 1, chip] = jnp.where(low, 0.0, q).astype(BF16)
        pin[chip] = proj[:, 2 * qc + vc :].astype(BF16).astype(F32)

    halo_src[...] = pin[n_fs - 1, chip_rows - HALO :, :].astype(BF16)
    halo_copy = pltpu.make_async_remote_copy(
        halo_src, halo, halo_send, halo_recv, device_id=(s + 1, f, t), device_id_type=MESH,
    )

    @pl.when(s < n_sp - 1)
    def _():
        halo_copy.start()

    def fold(p):
        acc = p[:, :128]
        for i in range(1, p.shape[1] // 128):
            acc = acc + p[:, i * 128 : (i + 1) * 128]
        return acc

    def attend(j, diagonal):
        for h in range(heads):
            keys = kv[j, :, :, h * pair : (h + 1) * pair].reshape(own_rows, pair)
            vals = kv[j, :, :, qc + h * v_dim : qc + (h + 1) * v_dim].reshape(own_rows, v_dim)
            for c in range(2):
                q = qhat[h, c].reshape(own_rows, pair)
                p = jnp.exp(
                    lax.dot_general(q, keys, (((1,), (1,)), ((), ())), preferred_element_type=F32)
                )
                if diagonal:
                    r = lax.broadcasted_iota(jnp.int32, p.shape, 0)
                    col = lax.broadcasted_iota(jnp.int32, p.shape, 1)
                    p = jnp.where(col <= r, p, 0.0)
                pv = jnp.dot(p.astype(BF16), vals, preferred_element_type=F32)
                if diagonal:
                    numer[h, c] = pv
                    total[h, c] = fold(p)
                else:
                    numer[h, c] += pv
                    total[h, c] += fold(p)

    relay(1, 1)
    relay(1, 2)
    relay(2, 0)
    attend(s, True)
    relay(2, 1)
    relay(3, 0)

    @pl.when(s > 0)
    def _():
        halo_copy.wait_recv()

    @pl.when(s == 0)
    def _():
        halo[...] = jnp.zeros_like(halo)

    group = ((f * 2 + t) * pc) // POOL_GROUP_DIM
    ext = jnp.concatenate([halo[...].astype(F32), pin[...].reshape(own_rows, pc)], axis=0)
    gvec = jnp.full(ext.shape, group, jnp.int32)
    window = ext + pltpu.roll(ext, 1, 0)
    chosen = window
    for i, shift in enumerate((2, 4, 8)):
        window = window + pltpu.roll(window, shift, 0)
        chosen = jnp.where(gvec > i, window, chosen)
    chosen = chosen[HALO:]
    pos = s * own_rows + lax.broadcasted_iota(jnp.int32, (own_rows, pc), 0)
    size = jnp.left_shift(jnp.full((own_rows, pc), 2, jnp.int32), gvec[HALO:])
    divisor = jnp.minimum(pos + 1, size).astype(F32)
    pooled = (chosen / divisor - ext[HALO:]).astype(BF16)
    merged[:, :, :, vc:] = pooled.reshape(n_fs, 2, rows, pc)

    def earlier(d, carry):
        j = s - d
        for k in range(last, -1, -1):
            relay(d + last - k, k)
        attend(j, False)
        return carry

    lax.fori_loop(1, s + 1, earlier, 0)

    for h in range(heads):
        first = numer[h, 0] / jnp.sum(total[h, 0], axis=-1, keepdims=True)
        second = numer[h, 1] / jnp.sum(total[h, 1], axis=-1, keepdims=True)
        o = first - lambdas_ref[h] * second
        o = o * lax.rsqrt(jnp.mean(o * o, axis=-1, keepdims=True) + EPS) * head_gain_ref[...]
        merged[:, :, :, h * v_dim : (h + 1) * v_dim] = o.astype(BF16).reshape(
            n_fs, 2, rows, v_dim
        )

    for c in wout_copies:
        c.wait()
    depth = vc + pc
    cw = out_ref.shape[1] // col_chunks
    theirs = merged[:, 1 - t].reshape(n_fs * rows, depth)
    mine = merged[:, t].reshape(n_fs * rows, depth)
    a_copies = []
    for n in range(col_chunks):
        y = jnp.dot(theirs, wout[:, n * cw : (n + 1) * cw], preferred_element_type=F32)
        part_send[n] = y.astype(BF16)
        c = pltpu.make_async_remote_copy(
            part_send.at[n], part_recv.at[n], a_send.at[n], a_recv.at[n],
            device_id=mate, device_id_type=MESH,
        )
        c.start()
        a_copies.append(c)
    b_copies = []
    for n in range(col_chunks):
        y = jnp.dot(mine, wout[:, n * cw : (n + 1) * cw], preferred_element_type=F32)
        a_copies[n].wait_recv()
        y = y + part_recv[n].astype(F32)
        chip_own[n] = y.reshape(n_fs, rows, cw)
        chip_send[n] = y.astype(BF16).reshape(n_fs, rows, cw)
        near = chips[1 + n % 2]
        steps = []
        for i, (ref, to) in enumerate((
            (chip_send.at[n, chips[last]], near),
            (chip_send.at[n, near], near),
            (chip_relay.at[n], chips[2 - n % 2]),
        )):
            steps.append(pltpu.make_async_remote_copy(
                ref, chip_recv.at[n, i], b_send.at[n, i], b_recv.at[n, i],
                device_id=(s, to, t), device_id_type=MESH,
            ))
        steps[0].start()
        steps[1].start()
        b_copies.append(steps)
    for n in range(col_chunks):
        b_copies[n][0].wait_recv()
        y = chip_own[n, chips[2 - n % 2]] + chip_recv[n, 0].astype(F32)
        chip_relay[n] = y.astype(BF16)
        b_copies[n][2].start()
    for n in range(col_chunks):
        b_copies[n][1].wait_recv()
        y = chip_own[n, f] + chip_recv[n, 1].astype(F32)
        b_copies[n][2].wait_recv()
        out_ref[:, n * cw : (n + 1) * cw] = (y + chip_recv[n, 2].astype(F32)).astype(BF16)

    for c in own[0] + own[1] + far + sum(forwards, []) + a_copies + sum(b_copies, []):
        c.wait_send()

    @pl.when(s < n_sp - 1)
    def _():
        halo_copy.wait_send()

        def drain(j, carry):
            for k in range(n_fs):
                kv_copy(j, k).wait_send()
            return carry

        lax.fori_loop(0, s + 1, drain, 0)


def solution(mesh):
    n_sp, n_fs, n_tp = mesh.shape["sp"], mesh.shape["fs"], mesh.shape["tp"]
    assert n_tp == 2 and n_fs == 4

    def body(tokens, norm_gain, w_query, w_key, w_value, w_pool, query_gain, key_gain,
             lambdas, head_gain, w_out_attn, w_out_pool):
        rows, width = tokens.shape
        out_width = w_out_attn.shape[1]
        heads = lambdas.shape[0]
        qc, vc, pc = w_query.shape[1], w_value.shape[1], w_pool.shape[1]
        v_dim = head_gain.shape[0]
        chip_rows = 2 * rows
        own_rows = n_fs * chip_rows
        col_chunks = 4
        cw = out_width // col_chunks
        hbm = pl.BlockSpec(memory_space=pl.ANY)
        vmem = pl.BlockSpec(memory_space=pltpu.VMEM)
        smem = pl.BlockSpec(memory_space=pltpu.SMEM)
        dma = pltpu.SemaphoreType.DMA
        return pl.pallas_call(
            functools.partial(kernel, n_sp, n_fs, col_chunks),
            out_shape=pltpu.VMEM((rows, out_width), BF16),
            in_specs=[hbm, vmem, hbm, hbm, hbm, hbm, vmem, vmem, smem, vmem, hbm, hbm],
            out_specs=vmem,
            scratch_shapes=[
                pltpu.VMEM((rows, width), BF16),
                pltpu.VMEM((n_fs, 2, 2, rows // 2, width), BF16),
                pltpu.VMEM((width, 2 * qc + vc + pc), BF16),
                pltpu.VMEM((vc + pc, out_width), BF16),
                pltpu.VMEM((n_sp, n_fs, chip_rows, qc + vc), BF16),
                pltpu.VMEM((heads, 2, n_fs, chip_rows, 2 * HEAD_DIM), BF16),
                pltpu.VMEM((n_fs, chip_rows, pc), F32),
                pltpu.VMEM((HALO, pc), BF16),
                pltpu.VMEM((HALO, pc), BF16),
                pltpu.VMEM((heads, 2, own_rows, v_dim), F32),
                pltpu.VMEM((heads, 2, own_rows, 128), F32),
                pltpu.VMEM((n_fs, 2, rows, vc + pc), BF16),
                pltpu.VMEM((col_chunks, n_fs * rows, cw), BF16),
                pltpu.VMEM((col_chunks, n_fs * rows, cw), BF16),
                pltpu.VMEM((col_chunks, n_fs, rows, cw), F32),
                pltpu.VMEM((col_chunks, n_fs, rows, cw), BF16),
                pltpu.VMEM((col_chunks, rows, cw), BF16),
                pltpu.VMEM((col_chunks, 3, rows, cw), BF16),
                dma(()), dma((4,)), dma((2,)),
                dma((2, 3)), dma((2, 3)), dma((n_fs, 2)), dma((n_fs, 2)),
                dma((n_sp, n_fs)), dma((n_sp, n_fs)),
                dma(()), dma(()),
                dma((col_chunks,)), dma((col_chunks,)),
                dma((col_chunks, 3)), dma((col_chunks, 3)),
            ],
            compiler_params=pltpu.CompilerParams(
                collective_id=0, has_side_effects=True, vmem_limit_bytes=60 * 1024 * 1024
            ),
        )(tokens, norm_gain.reshape(1, -1), w_query, w_key, w_value, w_pool,
          query_gain.reshape(1, -1), key_gain.reshape(1, -1), lambdas,
          head_gain.reshape(1, -1), w_out_attn, w_out_pool)

    cols = P(None, ("fs", "tp"))
    flat = P(("fs", "tp"), None)
    return jax.shard_map(
        body,
        mesh=mesh,
        in_specs=(P(("sp", "fs", "tp"), None), P(), cols, cols, cols, cols, P(), P(),
                  P(("fs", "tp")), P(), flat, flat),
        out_specs=P(("sp", "fs", "tp"), None),
        check_vma=False,
    )
```

profile of v0, /device:TPU:25, one launch (start us, length us, event | category | flops | bytes accessed | tf_op | source)
XLA Modules:
  0.0 30.7 jit_solution(4972959535422052668)
XLA Ops:
  0.7 29.4 %shard_map.118 = bf16[32,2048]{1,0:T(8,128)(2,1)S(1)} custom-call(bf16[32,2048]{1,0:T(8,128)(2,1)} %tokens_hbm.1, f32[1,2048]{1,0:T(1,128)} %bitcast.4, bf16[2048,128]{1,0:T(8,128)(2,1)} %wq_hbm.1, bf16[2048,128]{1,0:T(8,128)(2,1)} %wk_hbm.1, bf16[2048,128]{1,0:T(8,128)(2,1)} %wv_hbm.1, bf16[2048,128]{1,0:T(8,128)(2,1)} %wp_hbm.1, f32[1,64]{1,0:T(1,128)} %bitcast.5, ...), custom_call_target="tpu_custom_call" | custom-call | tf_op jit(solution)/shard_map/pallas_call | solution.py:349
  30.0 0.7 %copy.14 = bf16[32,2048]{1,0:T(8,128)(2,1)} copy(bf16[32,2048]{1,0:T(8,128)(2,1)S(1)} %shard_map.118) | data formatting | bytes 262144
where the time goes:
time: 31 us; the launch traced here: 30.7 us
  Pallas kernels  29.4 us (95%)
  local copies, waits for them, and re-layouts  0.66 us (2%)
  between operations  0.66 us (2%)
    pallas_call x1, Pallas kernels, body(): pl.pallas_call(functools.partial(kernel, n_sp, n_fs, col_chunks), out_sha...  29.4 us
    unnamed x1, local copies, waits for them, and re-layouts  0.66 us

commit v1 on v0

--- a/solution.py
+++ b/solution.py
@@ -18,13 +18,14 @@
 
 def kernel(
     n_sp, n_fs, col_chunks,
-    tokens_hbm, norm_gain_ref, wq_hbm, wk_hbm, wv_hbm, wp_hbm, query_gain_ref, key_gain_ref,
-    lambdas_ref, head_gain_ref, woa_hbm, wop_hbm,
+    tokens_hbm, norm_gain_hbm, wq_hbm, wk_hbm, wv_hbm, wp_hbm, query_gain_hbm, key_gain_hbm,
+    lambdas_hbm, head_gain_hbm, woa_hbm, wop_hbm,
     out_ref,
+    norm_gain_ref, query_gain_ref, key_gain_ref, lambdas_ref, head_gain_ref,
     tok, gathered, win, wout, kv, qhat, pin, halo_src, halo, numer, total, merged,
     part_send, part_recv, chip_own, chip_send, chip_relay, chip_recv,
-    tok_sem, win_sem, wout_sem, ag_send, ag_recv, fwd_send, fwd_recv, kv_send, kv_recv,
-    halo_send, halo_recv, a_send, a_recv, b_send, b_recv,
+    small_sem, tok_sem, win_sem, wout_sem, send_sem, ag_recv, fwd_recv, kv_send, kv_recv,
+    halo_send, halo_recv, a_recv, b_recv,
 ):
     s = lax.axis_index("sp")
     f = lax.axis_index("fs")
@@ -33,7 +34,7 @@
     rows, width = tok.shape
     chip_rows = 2 * rows
     own_rows = n_fs * chip_rows
-    heads = lambdas_ref.shape[0]
+    heads = lambdas_ref.shape[1]
     qc = wq_hbm.shape[1]
     vc = wv_hbm.shape[1]
     pc = wp_hbm.shape[1]
@@ -62,18 +63,29 @@
     def _():
         pl.semaphore_signal(barrier, inc=1, device_id=(s + 1, f, t), device_id_type=MESH)
 
+    small_copies = [
+        pltpu.make_async_copy(src, dst, small_sem.at[i])
+        for i, (src, dst) in enumerate((
+            (norm_gain_hbm, norm_gain_ref), (query_gain_hbm, query_gain_ref),
+            (key_gain_hbm, key_gain_ref), (lambdas_hbm, lambdas_ref),
+            (head_gain_hbm, head_gain_ref),
+        ))
+    ]
+    for c in small_copies:
+        c.start()
     win_copies = []
     at = 0
-    for i, (w, c) in enumerate(((wk_hbm, qc), (wv_hbm, vc), (wq_hbm, qc), (wp_hbm, pc))):
-        win_copies.append(pltpu.make_async_copy(w, win.at[:, pl.ds(at, c)], win_sem.at[i]))
+    for w, c in ((wk_hbm, qc), (wv_hbm, vc), (wq_hbm, qc), (wp_hbm, pc)):
+        win_copies.append(pltpu.make_async_copy(w, win.at[:, pl.ds(at, c)], win_sem))
         at += c
     wout_copies = [
-        pltpu.make_async_copy(woa_hbm, wout.at[pl.ds(0, vc), :], wout_sem.at[0]),
-        pltpu.make_async_copy(wop_hbm, wout.at[pl.ds(vc, pc), :], wout_sem.at[1]),
+        pltpu.make_async_copy(woa_hbm, wout.at[pl.ds(0, vc), :], wout_sem),
+        pltpu.make_async_copy(wop_hbm, wout.at[pl.ds(vc, pc), :], wout_sem),
     ]
     for c in win_copies + wout_copies:
         c.start()
 
+    small_copies[0].wait()
     tok_copy.wait()
     x = tok[...].astype(F32)
     x = x * lax.rsqrt(jnp.mean(x * x, axis=-1, keepdims=True) + EPS) * norm_gain_ref[...]
@@ -86,7 +98,7 @@
     def along(way, i, chip, half):
         slot = gathered.at[chip, t, half]
         return pltpu.make_async_remote_copy(
-            slot, slot, ag_send.at[way, i], ag_recv.at[way, i],
+            slot, slot, send_sem, ag_recv.at[way, i],
             device_id=(s, (fx, fy)[way], t), device_id_type=MESH,
         )
 
@@ -98,7 +110,7 @@
     def across(k, half):
         slot = gathered.at[chips[k], t, half]
         return pltpu.make_async_remote_copy(
-            slot, slot, fwd_send.at[k, half], fwd_recv.at[k, half],
+            slot, slot, send_sem, fwd_recv.at[k, half],
             device_id=mate, device_id_type=MESH,
         )
 
@@ -115,6 +127,8 @@
         second = jnp.sum(jnp.where(low, 0.0, sq), axis=-1, keepdims=True) * (1.0 / HEAD_DIM)
         return raw * jnp.where(low, lax.rsqrt(first + EPS), lax.rsqrt(second + EPS)) * gain
 
+    for c in small_copies[1:]:
+        c.wait()
     qg = jnp.concatenate([query_gain_ref[...]] * 2, axis=1)
     kg = jnp.concatenate([key_gain_ref[...]] * 2, axis=1)
 
@@ -123,7 +137,7 @@
     def kv_copy(j, k):
         slot = kv.at[j, chips[k]]
         return pltpu.make_async_remote_copy(
-            slot, slot, kv_send.at[j, k], kv_recv.at[j, k],
+            slot, slot, kv_send.at[j], kv_recv.at[j, k],
             device_id=(s + 1, f, t), device_id_type=MESH,
         )
 
@@ -158,10 +172,9 @@
         for c in forwards[k]:
             c.wait_recv()
         if k == 0:
-            for c in win_copies:
-                c.wait()
+            pltpu.make_async_copy(win, win, win_sem).wait()
         block = gathered[chip].reshape(chip_rows, width)
-        proj = jnp.dot(block, win[...], preferred_element_type=F32)
+        proj = jnp.dot(block, win[:, : qc + vc], preferred_element_type=F32)
         for h in range(heads):
             kv[s, chip, :, h * pair : (h + 1) * pair] = norm_pair(
                 proj[:, h * pair : (h + 1) * pair], kg
@@ -172,13 +185,14 @@
         def _(k=k):
             kv_copy(s, k).start()
 
+        proj = jnp.dot(block, win[:, qc + vc :], preferred_element_type=F32)
         for h in range(heads):
-            at = qc + vc + h * pair
+            at = h * pair
             q = norm_pair(proj[:, at : at + pair], qg)
             q = q.astype(BF16).astype(F32) * HEAD_DIM ** (-0.5)
             qhat[h, 0, chip] = jnp.where(low, q, 0.0).astype(BF16)
             qhat[h, 1, chip] = jnp.where(low, 0.0, q).astype(BF16)
-        pin[chip] = proj[:, 2 * qc + vc :].astype(BF16).astype(F32)
+        pin[chip] = proj[:, qc:].astype(BF16).astype(F32)
 
     halo_src[...] = pin[n_fs - 1, chip_rows - HALO :, :].astype(BF16)
     halo_copy = pltpu.make_async_remote_copy(
@@ -258,14 +272,13 @@
     for h in range(heads):
         first = numer[h, 0] / jnp.sum(total[h, 0], axis=-1, keepdims=True)
         second = numer[h, 1] / jnp.sum(total[h, 1], axis=-1, keepdims=True)
-        o = first - lambdas_ref[h] * second
+        o = first - lambdas_ref[0, h] * second
         o = o * lax.rsqrt(jnp.mean(o * o, axis=-1, keepdims=True) + EPS) * head_gain_ref[...]
         merged[:, :, :, h * v_dim : (h + 1) * v_dim] = o.astype(BF16).reshape(
             n_fs, 2, rows, v_dim
         )
 
-    for c in wout_copies:
-        c.wait()
+    pltpu.make_async_copy(wout, wout, wout_sem).wait()
     depth = vc + pc
     cw = out_ref.shape[1] // col_chunks
     theirs = merged[:, 1 - t].reshape(n_fs * rows, depth)
@@ -275,7 +288,7 @@
         y = jnp.dot(theirs, wout[:, n * cw : (n + 1) * cw], preferred_element_type=F32)
         part_send[n] = y.astype(BF16)
         c = pltpu.make_async_remote_copy(
-            part_send.at[n], part_recv.at[n], a_send.at[n], a_recv.at[n],
+            part_send.at[n], part_recv.at[n], send_sem, a_recv.at[n],
             device_id=mate, device_id_type=MESH,
         )
         c.start()
@@ -295,7 +308,7 @@
             (chip_relay.at[n], chips[2 - n % 2]),
         )):
             steps.append(pltpu.make_async_remote_copy(
-                ref, chip_recv.at[n, i], b_send.at[n, i], b_recv.at[n, i],
+                ref, chip_recv.at[n, i], send_sem, b_recv.at[n, i],
                 device_id=(s, to, t), device_id_type=MESH,
             ))
         steps[0].start()
@@ -312,16 +325,19 @@
         b_copies[n][2].wait_recv()
         out_ref[:, n * cw : (n + 1) * cw] = (y + chip_recv[n, 2].astype(F32)).astype(BF16)
 
-    for c in own[0] + own[1] + far + sum(forwards, []) + a_copies + sum(b_copies, []):
-        c.wait_send()
+    sent = (len(own[0] + own[1] + far) + 2 * n_fs) * (rows // 2) * width
+    sent += (col_chunks * n_fs + col_chunks * 3) * rows * cw
+    depth_words = win.shape[1]
+    assert sent % depth_words == 0 and sent // depth_words <= width
+    drained = win.at[pl.ds(0, sent // depth_words), :]
+    pltpu.make_async_copy(drained, drained, send_sem).wait()
 
     @pl.when(s < n_sp - 1)
     def _():
         halo_copy.wait_send()
 
         def drain(j, carry):
-            for k in range(n_fs):
-                kv_copy(j, k).wait_send()
+            pltpu.make_async_copy(kv.at[j], kv.at[j], kv_send.at[j]).wait()
             return carry
 
         lax.fori_loop(0, s + 1, drain, 0)
@@ -344,14 +360,18 @@
         cw = out_width // col_chunks
         hbm = pl.BlockSpec(memory_space=pl.ANY)
         vmem = pl.BlockSpec(memory_space=pltpu.VMEM)
-        smem = pl.BlockSpec(memory_space=pltpu.SMEM)
         dma = pltpu.SemaphoreType.DMA
         return pl.pallas_call(
             functools.partial(kernel, n_sp, n_fs, col_chunks),
             out_shape=pltpu.VMEM((rows, out_width), BF16),
-            in_specs=[hbm, vmem, hbm, hbm, hbm, hbm, vmem, vmem, smem, vmem, hbm, hbm],
+            in_specs=[hbm] * 12,
             out_specs=vmem,
             scratch_shapes=[
+                pltpu.VMEM((1, width), F32),
+                pltpu.VMEM((1, HEAD_DIM), F32),
+                pltpu.VMEM((1, HEAD_DIM), F32),
+                pltpu.SMEM((1, heads), F32),
+                pltpu.VMEM((1, v_dim), F32),
                 pltpu.VMEM((rows, width), BF16),
                 pltpu.VMEM((n_fs, 2, 2, rows // 2, width), BF16),
                 pltpu.VMEM((width, 2 * qc + vc + pc), BF16),
@@ -370,18 +390,17 @@
                 pltpu.VMEM((col_chunks, n_fs, rows, cw), BF16),
                 pltpu.VMEM((col_chunks, rows, cw), BF16),
                 pltpu.VMEM((col_chunks, 3, rows, cw), BF16),
-                dma(()), dma((4,)), dma((2,)),
-                dma((2, 3)), dma((2, 3)), dma((n_fs, 2)), dma((n_fs, 2)),
-                dma((n_sp, n_fs)), dma((n_sp, n_fs)),
+                dma((5,)), dma(()), dma(()), dma(()), dma(()),
+                dma((2, 3)), dma((n_fs, 2)),
+                dma((n_sp,)), dma((n_sp, n_fs)),
                 dma(()), dma(()),
-                dma((col_chunks,)), dma((col_chunks,)),
-                dma((col_chunks, 3)), dma((col_chunks, 3)),
+                dma((col_chunks,)), dma((col_chunks, 3)),
             ],
             compiler_params=pltpu.CompilerParams(
                 collective_id=0, has_side_effects=True, vmem_limit_bytes=60 * 1024 * 1024
             ),
         )(tokens, norm_gain.reshape(1, -1), w_query, w_key, w_value, w_pool,
-          query_gain.reshape(1, -1), key_gain.reshape(1, -1), lambdas,
+          query_gain.reshape(1, -1), key_gain.reshape(1, -1), lambdas.reshape(1, -1),
           head_gain.reshape(1, -1), w_out_attn, w_out_pool)
 
     cols = P(None, ("fs", "tp"))

time: 31 us -> 30 us (0.968)
  Pallas kernels: 29.4 us -> 28.4 us
    pallas_call x1, Pallas kernels: 29.4 us -> 28.4 us  [body(): pl.pallas_call(functools.partial(kernel, n_sp, n_fs, col_chunks), out_sha...]
where the time goes in v1:
time: 30 us; the launch traced here: 29.7 us
  Pallas kernels  28.4 us (95%)
  local copies, waits for them, and re-layouts  0.66 us (2%)
  between operations  0.66 us (2%)
    pallas_call x1, Pallas kernels, body(): pl.pallas_call(functools.partial(kernel, n_sp, n_fs, col_chunks), out_sha...  28.4 us
    unnamed x1, local copies, waits for them, and re-layouts  0.66 us

profile of v1, /device:TPU:25, one launch (start us, length us, event | category | flops | bytes accessed | tf_op | source)
XLA Modules:
  0.0 29.7 jit_solution(4360407309175214716)
XLA Ops:
  0.7 28.4 %shard_map.118 = bf16[32,2048]{1,0:T(8,128)(2,1)S(1)} custom-call(bf16[32,2048]{1,0:T(8,128)(2,1)} %tokens_hbm.1, f32[1,2048]{1,0:T(1,128)} %bitcast.6, bf16[2048,128]{1,0:T(8,128)(2,1)} %wq_hbm.1, bf16[2048,128]{1,0:T(8,128)(2,1)} %wk_hbm.1, bf16[2048,128]{1,0:T(8,128)(2,1)} %wv_hbm.1, bf16[2048,128]{1,0:T(8,128)(2,1)} %wp_hbm.1, f32[1,64]{1,0:T(1,128)} %bitcast.7, ...), custom_call_target="tpu_custom_call" | custom-call | tf_op jit(solution)/shard_map/pallas_call | solution.py:364
  29.0 0.7 %copy.14 = bf16[32,2048]{1,0:T(8,128)(2,1)} copy(bf16[32,2048]{1,0:T(8,128)(2,1)S(1)} %shard_map.118) | data formatting | bytes 262144
